TPU v7x, 32 devices: a whole 2x2x4 slice. The times are simulated.
32 devices in a mesh: tp: 16 (over z, y, x), dp: 2 (over core).
Axes of the slice: x: 2, y: 2, z: 4, core: 2. Of those that a mesh axis runs over, the one named last changes fastest.
Arguments:
- hidden: bfloat16 [16, 4096], P(None, 'dp'), may hold values from -6 to 6
- norm_gain: float32 [2, 4096], P(None, 'dp'), may hold values from 0.1 to 1.9
- gate_weight: bfloat16 [2, 4096, 8192], P(None, 'dp', 'tp'), may hold values from -0.09375 to 0.09375
- inner_weight: bfloat16 [2, 4096, 8192], P(None, 'dp', 'tp'), may hold values from -0.09375 to 0.09375
- write_weight: bfloat16 [2, 4096, 2048], P(None, 'dp', 'tp'), may hold values from -0.09375 to 0.09375
- read_weight: bfloat16 [2, 4096, 2048], P(None, 'dp', 'tp'), may hold values from -0.09375 to 0.09375
- step_weight: bfloat16 [2, 4096, 128], P(None, 'dp'), may hold values from -0.09375 to 0.09375
- conv_inner: bfloat16 [2, 4, 8192], P(None, None, 'tp'), may hold values from -3 to 3
- conv_write: bfloat16 [2, 4, 2048], P(None, None, 'tp'), may hold values from -3 to 3
- conv_read: bfloat16 [2, 4, 2048], P(None, None, 'tp'), may hold values from -3 to 3
- step_bias: float32 [2, 128], P(None, 'tp'), may hold values from -4 to -1
- decay_log: float32 [2, 128], P(None, 'tp'), may hold values from -3 to 0.5
- skip_gain: float32 [2, 128], P(None, 'tp'), may hold values from 0.1 to 1.9
- group_gain: float32 [2, 8192], P(None, 'tp'), may hold values from 0.1 to 1.9
- out_weight: bfloat16 [2, 8192, 4096], P(None, 'tp', 'dp'), may hold values from -0.4 to 0.4
- state_inner: bfloat16 [2, 16, 3, 8192], P(None, 'dp', None, 'tp'), may hold values from -6 to 6
- state_write: bfloat16 [2, 16, 3, 2048], P(None, 'dp', None, 'tp'), may hold values from -6 to 6
- state_read: bfloat16 [2, 16, 3, 2048], P(None, 'dp', None, 'tp'), may hold values from -6 to 6
- recurrent: float32 [2, 16, 128, 64, 128], P(None, 'dp', 'tp'), may hold values from -1.2 to 1.2, as said below
Outputs:
- out_hidden: bfloat16 [16, 4096], P(None, 'dp')
- next_inner: bfloat16 [2, 16, 3, 8192], P(None, 'dp', None, 'tp')
- next_write: bfloat16 [2, 16, 3, 2048], P(None, 'dp', None, 'tp')
- next_read: bfloat16 [2, 16, 3, 2048], P(None, 'dp', None, 'tp')
- next_recurrent: float32 [2, 16, 128, 64, 128], P(None, 'dp', 'tp')
Inputs may be any that keep to these rules, and one draw needn't show every extreme that they name: recurrent states of order a tenth, with scales that differ between heads.
All inputs are finite; a program needn't handle non-finite values.
Results may differ from a plain program's by a relative error of at most 0.025.
Values may be sent and summed in bfloat16 or wider, within the bound.
A program may use at most 64 MiB of HBM per device.

v0:
```python
import jax
import jax.numpy as jnp
from jax import lax
from jax.sharding import PartitionSpec as P

D = 4096
HEADS = 128
GROUPS = 16


eps = 1e-06


def convolve(state, fresh_row, kernel):
    window = jnp.concatenate([state, fresh_row[:, None, :]], axis=1)
    summed = jnp.sum(window.astype(jnp.float32) * kernel.astype(jnp.float32)[None], axis=1)
    return (jax.nn.silu(summed), window[:, 1:])


def mixer_block(normed, number, weights):
    (
        gate_weight,
        inner_weight,
        write_weight,
        read_weight,
        step_weight,
        conv_inner,
        conv_write,
        conv_read,
        step_bias,
        decay_log,
        skip_gain,
        group_gain,
        out_weight,
        state_inner,
        state_write,
        state_read,
        recurrent,
    ) = weights

    def partial_of(weight):
        return jnp.dot(normed, weight[number], preferred_element_type=jnp.float32).astype(
            jnp.bfloat16
        )

    summed = (
        lax.psum_scatter(partial_of(gate_weight), "dp", scatter_dimension=0, tiled=True).astype(
            jnp.float32
        ),
        lax.psum_scatter(partial_of(inner_weight), "dp", scatter_dimension=0, tiled=True).astype(
            jnp.float32
        ),
        lax.psum_scatter(partial_of(write_weight), "dp", scatter_dimension=0, tiled=True).astype(
            jnp.float32
        ),
        lax.psum_scatter(partial_of(read_weight), "dp", scatter_dimension=0, tiled=True).astype(
            jnp.float32
        ),
        lax.psum_scatter(partial_of(step_weight), "dp", scatter_dimension=0, tiled=True).astype(
            jnp.float32
        ),
    )
    gate_raw, inner_raw, write_raw, read_raw, step_raw = [
        member.astype(jnp.bfloat16) for member in summed
    ]
    inner_act, next_inner = convolve(state_inner[number], inner_raw, conv_inner[number])
    write_act, next_write = convolve(state_write[number], write_raw, conv_write[number])
    read_act, next_read = convolve(state_read[number], read_raw, conv_read[number])
    write_all, read_all = (
        lax.all_gather(write_act.astype(jnp.bfloat16), "tp", axis=1, tiled=True),
        lax.all_gather(read_act.astype(jnp.bfloat16), "tp", axis=1, tiled=True),
    )
    heads_here = step_bias.shape[1]
    head_dim = recurrent.shape[3]
    state_dim = recurrent.shape[4]
    rows_here = inner_act.shape[0]
    first_head = lax.axis_index("tp") * heads_here
    group_index = first_head // (HEADS // GROUPS)
    write_grid = write_all.reshape(rows_here, state_dim, GROUPS)
    read_grid = read_all.reshape(rows_here, state_dim, GROUPS)
    write_vec = lax.dynamic_slice_in_dim(write_grid, group_index, 1, 2)[:, :, 0].astype(jnp.float32)
    read_vec = lax.dynamic_slice_in_dim(read_grid, group_index, 1, 2)[:, :, 0].astype(jnp.float32)
    step_own = lax.dynamic_slice_in_dim(step_raw, first_head, heads_here, 1)
    step_size = jax.nn.softplus(step_own.astype(jnp.float32) + step_bias[number][None, :])
    retain = jnp.exp(-step_size * jnp.exp(decay_log[number])[None, :])
    inner_heads = inner_act.reshape(rows_here, heads_here, head_dim)
    updated = (
        retain[:, :, None, None] * recurrent[number]
        + (step_size[:, :, None] * inner_heads)[:, :, :, None] * write_vec[:, None, None, :]
    )
    readout = jnp.einsum("bhpn,bn->bhp", updated, read_vec, precision=lax.Precision.HIGHEST)
    readout = readout + skip_gain[number][None, :, None] * inner_heads
    gated_out = readout.reshape(rows_here, heads_here * head_dim) * jax.nn.silu(
        gate_raw.astype(jnp.float32)
    )
    selector = (jnp.arange(GROUPS) == group_index).astype(jnp.float32)
    totals = lax.psum(jnp.sum(gated_out * gated_out, axis=1)[:, None] * selector[None, :], "tp")
    group_sum = jnp.sum(totals * selector[None, :], axis=1, keepdims=True)
    group_factor = lax.rsqrt(group_sum / (HEADS // GROUPS * head_dim) + eps)
    group_normed = (gated_out * group_factor * group_gain[number][None, :]).astype(jnp.bfloat16)
    branch = jnp.dot(
        lax.all_gather(group_normed, "dp", axis=0, tiled=True),
        out_weight[number],
        preferred_element_type=jnp.float32,
    )
    return (branch, (next_inner, next_write, next_read, updated))


def total_over(branch):
    return lax.psum(branch, "tp")


def local(
    hidden,
    norm_gain,
    gate_weight,
    inner_weight,
    write_weight,
    read_weight,
    step_weight,
    conv_inner,
    conv_write,
    conv_read,
    step_bias,
    decay_log,
    skip_gain,
    group_gain,
    out_weight,
    state_inner,
    state_write,
    state_read,
    recurrent,
):
    weights = (
        gate_weight,
        inner_weight,
        write_weight,
        read_weight,
        step_weight,
        conv_inner,
        conv_write,
        conv_read,
        step_bias,
        decay_log,
        skip_gain,
        group_gain,
        out_weight,
        state_inner,
        state_write,
        state_read,
        recurrent,
    )
    wide_in = hidden.astype(jnp.float32)
    squares = lax.psum(jnp.sum(wide_in * wide_in, axis=1, keepdims=True), "dp")
    normed = (wide_in * lax.rsqrt(squares / D + eps) * norm_gain[0][None, :]).astype(jnp.bfloat16)
    branch, first_states = mixer_block(normed, 0, weights)
    middle = (wide_in + total_over(branch)).astype(jnp.bfloat16).astype(jnp.float32)
    squares = lax.psum(jnp.sum(middle * middle, axis=1, keepdims=True), "dp")
    normed = (middle * lax.rsqrt(squares / D + eps) * norm_gain[1][None, :]).astype(jnp.bfloat16)
    branch, second_states = mixer_block(normed, 1, weights)
    result = (middle + total_over(branch)).astype(jnp.bfloat16)
    stacked = [jnp.stack([earlier, later]) for earlier, later in zip(first_states, second_states)]
    return (result, stacked[0], stacked[1], stacked[2], stacked[3])


def solution(mesh):
    return jax.shard_map(
        local,
        mesh=mesh,
        in_specs=(
            P(None, "dp"),
            P(None, "dp"),
            P(None, "dp", "tp"),
            P(None, "dp", "tp"),
            P(None, "dp", "tp"),
            P(None, "dp", "tp"),
            P(None, "dp", None),
            P(None, None, "tp"),
            P(None, None, "tp"),
            P(None, None, "tp"),
            P(None, "tp"),
            P(None, "tp"),
            P(None, "tp"),
            P(None, "tp"),
            P(None, "tp", "dp"),
            P(None, "dp", None, "tp"),
            P(None, "dp", None, "tp"),
            P(None, "dp", None, "tp"),
            P(None, "dp", "tp", None, None),
        ),
        out_specs=(
            P(None, "dp"),
            P(None, "dp", None, "tp"),
            P(None, "dp", None, "tp"),
            P(None, "dp", None, "tp"),
            P(None, "dp", "tp", None, None),
        ),
        check_vma=False,
    )
```

profile of v0, /device:TPU:0, one launch (start us, length us, event | category | flops | bytes accessed | tf_op | source)
XLA Modules:
  0.0 509.0 jit_solution(9227752754220769065)
XLA Ops:
  7.2 1.0 fusion.58
  8.2 2.6 psum.42
  10.8 0.8 fusion.97
  11.8 2.8 fusion.28
  14.7 2.6 fusion.31
  17.4 0.6 dynamic-slice
  18.8 0.2 convolution_convert_fusion.4
  19.1 0.2 convolution_convert_fusion.3
  19.3 1.3 convolution_convert_fusion.5
  20.6 3.5 all-reduce.7
  24.2 42.2 %all_gather.18 = bf16[8,2048]{1,0:T(8,128)(2,1)S(1)} all-gather(bf16[8,128]{1,0:T(8,128)(2,1)S(1)} %multiply_convert_fusion.5), channel_id=1, replica_groups=mesh['tp'=16,'dp'=2] {'tp'}, dimensions={1}, use_global_device_ids=true | all-gather | bytes 34816 | tf_op jit(solution)/shard_map/all_gather | solution.py:70
  66.4 35.6 %all_gather.19 = bf16[8,2048]{1,0:T(8,128)(2,1)S(1)} all-gather(bf16[8,128]{1,0:T(8,128)(2,1)S(1)} %multiply_convert_fusion.4), channel_id=1, replica_groups=mesh['tp'=16,'dp'=2] {'tp'}, dimensions={1}, use_global_device_ids=true | all-gather | bytes 34816 | tf_op jit(solution)/shard_map/all_gather | solution.py:71
  102.2 0.3 dynamic-slice_reduce_fusion.1
  102.7 0.2 convert_reduce_fusion.1
  103.2 0.7 multiply_reduce_fusion.1
  104.0 4.2 fusion.16
  108.4 0.8 multiply_reduce_fusion.5
  109.3 38.6 %psum.43 = f32[8,16]{1,0:T(8,128)S(1)} all-reduce(f32[8,16]{1,0:T(8,128)S(1)} %broadcast_multiply_fusion.3), channel_id=1, replica_groups=mesh['tp'=16,'dp'=2] {'tp'}, use_global_device_ids=true, to_apply=%region_11.12 | all-reduce | flops 128 | bytes 1024 | tf_op jit(solution)/shard_map/psum | solution.py:97
  148.0 0.8 multiply_convert_fusion.1
  148.8 1.8 all_gather.20
  150.6 2.6 fusion.9
  153.4 101.5 %all-reduce.11.cloned.1.call-done = f32[16,2048]{1,0:T(8,128)} async-done(((f32[16,2048]{1,0:T(8,128)}), f32[16,2048]{1,0:T(8,128)}) %all-reduce.11.cloned.1.call-update) | async-done | bytes 131088 | tf_op jit(solution)/shard_map/psum | solution.py:110
  254.8 1.0 fusion.62
  255.9 2.5 psum.45
  258.4 0.2 convolution_convert_fusion.1
  258.6 0.2 convolution_convert_fusion
  258.8 1.3 convolution_convert_fusion.2
  260.1 2.6 fusion.34
  262.8 2.6 fusion.37
  265.4 3.3 all-reduce.6
  268.8 0.6 pad_maximum_fusion.4
  269.5 0.6 pad_maximum_fusion.5
  270.1 38.9 %all_gather.21 = bf16[8,2048]{1,0:T(8,128)(2,1)S(1)} all-gather(bf16[8,128]{1,0:T(8,128)(2,1)S(1)} %multiply_convert_fusion.3), channel_id=1, replica_groups=mesh['tp'=16,'dp'=2] {'tp'}, dimensions={1}, use_global_device_ids=true | all-gather | bytes 34816 | tf_op jit(solution)/shard_map/all_gather | solution.py:70
  309.1 35.6 %all_gather.22 = bf16[8,2048]{1,0:T(8,128)(2,1)S(1)} all-gather(bf16[8,128]{1,0:T(8,128)(2,1)S(1)} %multiply_convert_fusion.2), channel_id=1, replica_groups=mesh['tp'=16,'dp'=2] {'tp'}, dimensions={1}, use_global_device_ids=true | all-gather | bytes 34816 | tf_op jit(solution)/shard_map/all_gather | solution.py:71
  345.0 0.3 dynamic-slice_reduce_fusion
  345.3 0.3 convert_reduce_fusion
  345.7 0.7 multiply_reduce_fusion
  346.6 4.2 multiply_add_fusion.1
  350.8 2.8 fusion.7
  353.8 0.8 multiply_reduce_fusion.2
  354.7 39.1 %psum.46 = f32[8,16]{1,0:T(8,128)S(1)} all-reduce(f32[8,16]{1,0:T(8,128)S(1)} %broadcast_multiply_fusion.2), channel_id=1, replica_groups=mesh['tp'=16,'dp'=2] {'tp'}, use_global_device_ids=true, to_apply=%region_25.26 | all-reduce | flops 128 | bytes 1024 | tf_op jit(solution)/shard_map/psum | solution.py:97
  393.9 0.8 multiply_convert_fusion
  394.7 1.8 all_gather.23
  396.5 2.6 fusion
  399.1 4.1 pad_maximum_fusion
  403.2 0.6 pad_maximum_fusion.1
  403.8 96.8 %all-reduce.13.cloned.1.call-done = f32[16,2048]{1,0:T(8,128)} async-done(((f32[16,2048]{1,0:T(8,128)}), f32[16,2048]{1,0:T(8,128)}) %all-reduce.13.cloned.1.call-update) | async-done | bytes 131088 | tf_op jit(solution)/shard_map/psum | solution.py:110
  500.6 1.6 fusion.65
  (101 shorter events, 2.8 us)
Async XLA Ops:
  7.2 7.5 %copy-start.1 = (bf16[16,2048]{1,0:T(8,128)(2,1)S(1)}, bf16[16,2048]{1,0:T(8,128)(2,1)}, u32[]{:S(2)}) copy-start(bf16[16,2048]{1,0:T(8,128)(2,1)} %param.19) | copy-start | bytes 196612
  7.2 96.0 %reduce-scatter.5.cloned.1.call-start = ((), (), s32[]{:S(2)}) async-start(), calls=%async_computation.4 | async-start | bytes 24576 | tf_op jit(solution)/shard_map/reduce_scatter | solution.py:50
  11.7 5.8 %copy-start.16 = (u32[32]{0:T(128)S(1)}, u32[32]{0:T(128)}, u32[]{:S(2)}) copy-start(u32[32]{0:T(128)} %constant.63) | copy-start | bytes 388
  11.7 7.0 %copy-start.11 = (f32[2,8]{1,0:T(2,128)S(1)}, f32[2,8]{1,0:T(2,128)}, u32[]{:S(2)}) copy-start(f32[2,8]{1,0:T(2,128)} %param.31) | copy-start | bytes 196
  11.7 7.0 %copy-start.9 = (bf16[2,4,128]{2,1,0:T(4,128)(2,1)S(1)}, bf16[2,4,128]{2,1,0:T(4,128)(2,1)}, u32[]{:S(2)}) copy-start(bf16[2,4,128]{2,1,0:T(4,128)(2,1)} %param.27) | copy-start | bytes 6148
  11.7 7.0 %copy-start.10 = (bf16[2,4,128]{2,1,0:T(4,128)(2,1)S(1)}, bf16[2,4,128]{2,1,0:T(4,128)(2,1)}, u32[]{:S(2)}) copy-start(bf16[2,4,128]{2,1,0:T(4,128)(2,1)} %param.28) | copy-start | bytes 6148
  11.7 7.0 %copy-start.8 = (f32[2,512]{1,0:T(2,128)S(1)}, f32[2,512]{1,0:T(2,128)}, u32[]{:S(2)}) copy-start(f32[2,512]{1,0:T(2,128)} %param.32) | copy-start | bytes 12292
  11.7 7.1 %copy-start.5 = (bf16[2,8,3,128]{3,1,2,0:T(8,128)(2,1)S(1)}, bf16[2,8,3,128]{3,1,2,0:T(8,128)(2,1)}, u32[]{:S(2)}) copy-start(bf16[2,8,3,128]{3,1,2,0:T(8,128)(2,1)} %param.35) | copy-start | bytes 36868
  11.7 7.1 %copy-start.6 = (bf16[2,8,3,128]{3,1,2,0:T(8,128)(2,1)S(1)}, bf16[2,8,3,128]{3,1,2,0:T(8,128)(2,1)}, u32[]{:S(2)}) copy-start(bf16[2,8,3,128]{3,1,2,0:T(8,128)(2,1)} %param.36) | copy-start | bytes 36868
  11.7 7.1 %copy-start.14 = (bf16[2,2048,128]{2,1,0:T(8,128)(2,1)S(1)}, bf16[2,2048,128]{2,1,0:T(8,128)(2,1)}, u32[]{:S(2)}) copy-start(bf16[2,2048,128]{2,1,0:T(8,128)(2,1)} %param.23) | copy-start | bytes 3145732
  11.8 7.3 %copy-start.15 = (bf16[2,2048,128]{2,1,0:T(8,128)(2,1)S(1)}, bf16[2,2048,128]{2,1,0:T(8,128)(2,1)}, u32[]{:S(2)}) copy-start(bf16[2,2048,128]{2,1,0:T(8,128)(2,1)} %param.24) | copy-start | bytes 3145732
  14.6 9.5 %copy-start.7 = (bf16[2,4,512]{2,1,0:T(4,128)(2,1)S(1)}, bf16[2,4,512]{2,1,0:T(4,128)(2,1)}, u32[]{:S(2)}) copy-start(bf16[2,4,512]{2,1,0:T(4,128)(2,1)} %param.26) | copy-start | bytes 24580
  14.6 87.4 %copy-start.2 = (bf16[2,8,3,512]{3,1,2,0:T(8,128)(2,1)S(1)}, bf16[2,8,3,512]{3,1,2,0:T(8,128)(2,1)}, u32[]{:S(2)}) copy-start(bf16[2,8,3,512]{3,1,2,0:T(8,128)(2,1)} %param.34) | copy-start | bytes 147460
  14.6 93.8 %reduce-scatter.7.cloned.1.call-start = ((), (), s32[]{:S(2)}) async-start(), calls=%async_computation.5 | async-start | bytes 24576 | tf_op jit(solution)/shard_map/reduce_scatter | solution.py:47
  17.3 85.7 %copy-start.12 = (f32[2,8]{1,0:T(2,128)S(1)}, f32[2,8]{1,0:T(2,128)}, u32[]{:S(2)}) copy-start(f32[2,8]{1,0:T(2,128)} %param.30) | copy-start | bytes 196
  17.3 85.7 %copy-start.13 = (f32[2,8]{1,0:T(2,128)S(1)}, f32[2,8]{1,0:T(2,128)}, u32[]{:S(2)}) copy-start(f32[2,8]{1,0:T(2,128)} %param.29) | copy-start | bytes 196
  17.3 237.5 %all-reduce.11.cloned.1.call-start = ((), (), s32[]{:S(2)}) async-start(), calls=%async_computation.6 | async-start | bytes 262144 | tf_op jit(solution)/shard_map/psum | solution.py:110
  104.0 49.3 %copy-start.3 = (bf16[8,512]{1,0:T(8,128)(2,1)S(1)}, bf16[8,512]{1,0:T(8,128)(2,1)}, u32[]{:S(2)}) copy-start(bf16[8,512]{1,0:T(8,128)(2,1)} %reduce-scatter.5.cloned.1.call-done) | copy-start | bytes 24580
  153.3 192.4 %reduce-scatter.9.cloned.1.call-start = ((), (), s32[]{:S(2)}) async-start(), calls=%async_computation.7 | async-start | bytes 24576 | tf_op jit(solution)/shard_map/reduce_scatter | solution.py:50
  268.8 85.0 %reduce-scatter.11.cloned.1.call-start = ((), (), s32[]{:S(2)}) async-start(), calls=%async_computation.8 | async-start | bytes 24576 | tf_op jit(solution)/shard_map/reduce_scatter | solution.py:47
  345.5 155.1 %all-reduce.13.cloned.1.call-start = ((), (), s32[]{:S(2)}) async-start(), calls=%async_computation.9 | async-start | bytes 262144 | tf_op jit(solution)/shard_map/psum | solution.py:110
  346.6 4.2 copy-start
  399.1 4.1 copy-start.4
Sparse Core Ops, SparseCore 0:
  14.7 10.0 reduce-scatter.4
  27.6 8.6 reduce-scatter.6
  153.4 101.3 all-reduce.10
  268.9 6.5 reduce-scatter.8
  345.7 5.2 reduce-scatter.10
  399.3 101.3 all-reduce.12
where the time goes:
time: 510 us; the launch traced here: 509 us
  blocking collectives  245 us (48%)
  waiting for transfers between devices  198 us (39%)
  matrix products  26.6 us (5%)
  other arithmetic  19.8 us (4%)
  between operations  15.3 us (3%)
    psum x2, waiting for transfers between devices, total_over(): return lax.psum(branch, 'tp')  198 us
    all_gather x2, blocking collectives, mixer_block(): lax.all_gather(write_act.astype(jnp.bfloat16), 'tp', axis=1, tiled=True)  81.1 us
    psum x2, blocking collectives, mixer_block(): lax.psum(jnp.sum(gated_out * gated_out, axis=1)[:, None] * selector[None,...  77.7 us
    all_gather x2, blocking collectives, mixer_block(): lax.all_gather(read_act.astype(jnp.bfloat16), 'tp', axis=1, tiled=True)  71.2 us
    dot_general x10, matrix products, partial_of(): jnp.dot(normed, weight[number], preferred_element_type=jnp.float32)  14.2 us
  transfers between devices with their start and end apart: 6, of which 2 were waited for; matrix products, arithmetic and copies ran while one was open for 5% of the time, Pallas kernels for 0%

commit v1 on v0

--- a/solution.py
+++ b/solution.py
@@ -1,6 +1,8 @@
 import jax
 import jax.numpy as jnp
 from jax import lax
+from jax.experimental import pallas as pl
+from jax.experimental.pallas import tpu as pltpu
 from jax.sharding import PartitionSpec as P
 
 D = 4096
@@ -163,9 +165,383 @@
     return (result, stacked[0], stacked[1], stacked[2], stacked[3])
 
 
+def fused_kernel(
+    tp,
+    hidden_ref,
+    norm_gain_ref,
+    tap_ref,
+    pre_ref,
+    bias_ref,
+    decay_ref,
+    skip_ref,
+    group_gain_ref,
+    gate_hbm,
+    inner_hbm,
+    write_hbm,
+    read_hbm,
+    step_hbm,
+    out_hbm,
+    rec_hbm,
+    result_ref,
+    raw_ref,
+    retain_ref,
+    scaled_ref,
+    vec_ref,
+    gate_v,
+    inner_v,
+    small_v,
+    out_v,
+    rec_v,
+    pick_v,
+    spread_v,
+    part_a,
+    part_b,
+    got_a,
+    got_b,
+    gath,
+    normed_mine,
+    normed_peer,
+    branch_v,
+    red,
+    stream_v,
+    w_sem,
+    dp_send,
+    dp_recv,
+    gath_send,
+    gath_recv,
+    red_send,
+    red_recv,
+    str_send,
+    str_recv,
+):
+    t = lax.axis_index("tp")
+    me = lax.axis_index("dp")
+    peer = 1 - me
+    layers = norm_gain_ref.shape[0]
+    rows = hidden_ref.shape[0]
+    own = rows // 2
+    width = hidden_ref.shape[1]
+    total_width = width * 2
+    inner = gate_hbm.shape[2]
+    cols = write_hbm.shape[2]
+    step_cols = step_hbm.shape[2]
+    small = 2 * cols + step_cols
+    chunk = width // tp
+    heads = bias_ref.shape[1]
+    head_dim = inner // heads
+
+    def load(source, target, number):
+        return pltpu.make_async_copy(source, target, w_sem.at[number])
+
+    loads = []
+    for l in range(layers):
+        at = 7 * l
+        loads.append(
+            [
+                load(write_hbm.at[l], small_v.at[l, :, pl.ds(0, cols)], at),
+                load(read_hbm.at[l], small_v.at[l, :, pl.ds(cols, cols)], at + 1),
+                load(step_hbm.at[l], small_v.at[l, :, pl.ds(2 * cols, step_cols)], at + 2),
+                load(inner_hbm.at[l], inner_v.at[l], at + 3),
+                load(gate_hbm.at[l], gate_v.at[l], at + 4),
+                load(rec_hbm.at[l], rec_v.at[l], at + 5),
+                load(out_hbm.at[l], out_v.at[l], at + 6),
+            ]
+        )
+    for l in range(layers):
+        for one in loads[l]:
+            one.start()
+
+    barrier = pltpu.get_barrier_semaphore()
+
+    @pl.loop(1, tp)
+    def _(k):
+        pl.semaphore_signal(barrier, inc=1, device_id={"tp": lax.rem(t + k, tp), "dp": me})
+
+    pl.semaphore_signal(barrier, inc=1, device_id={"tp": t, "dp": peer})
+
+    big = pick_v.shape
+    pick_v[...] = (
+        lax.broadcasted_iota(jnp.int32, big, 0)
+        == lax.broadcasted_iota(jnp.int32, big, 1) * tp + t
+    ).astype(jnp.float32).astype(jnp.bfloat16)
+    grid = spread_v.shape
+    lane_head = lax.broadcasted_iota(jnp.int32, grid, 1) // head_dim
+    spread_v[...] = (
+        lax.broadcasted_iota(jnp.int32, grid, 0) == lane_head + heads * t
+    ).astype(jnp.float32).astype(jnp.bfloat16)
+
+    wide_head = lax.broadcasted_iota(jnp.int32, (own, inner), 1) // head_dim
+    own_row = lax.broadcasted_iota(jnp.int32, (own, inner), 0)
+
+    def widen(row):
+        wide = jnp.zeros((own, inner), jnp.float32)
+        for h in range(heads):
+            wide = jnp.where(
+                wide_head == h, jnp.broadcast_to(row[:, h : h + 1], (own, inner)), wide
+            )
+        return wide
+
+    bias_w = [widen(bias_ref[l : l + 1, :]) for l in range(layers)]
+    rate_w = [widen(jnp.exp(decay_ref[l : l + 1, :])) for l in range(layers)]
+    skip_w = [widen(skip_ref[l : l + 1, :]) for l in range(layers)]
+
+    def to_peer(source, target, number):
+        return pltpu.make_async_remote_copy(
+            src_ref=source,
+            dst_ref=target,
+            send_sem=dp_send.at[number],
+            recv_sem=dp_recv.at[number],
+            device_id={"tp": t, "dp": peer},
+        )
+
+    def spread_start(source_of, target, sends, recvs):
+        @pl.loop(1, tp)
+        def _(k):
+            to = lax.rem(t + k, tp)
+            pltpu.make_async_remote_copy(
+                src_ref=source_of(to),
+                dst_ref=target.at[t],
+                send_sem=sends.at[to],
+                recv_sem=recvs.at[t],
+                device_id={"tp": to, "dp": me},
+            ).start()
+
+    def spread_wait(source_of, target, sends, recvs):
+        @pl.loop(1, tp)
+        def _(k):
+            to = lax.rem(t + k, tp)
+            copy = pltpu.make_async_remote_copy(
+                src_ref=source_of(to),
+                dst_ref=target.at[to],
+                send_sem=sends.at[to],
+                recv_sem=recvs.at[to],
+                device_id={"tp": to, "dp": me},
+            )
+            copy.wait_send()
+            copy.wait_recv()
+
+    first = True
+    mine = pl.ds(pl.multiple_of(me * own, own), own)
+    theirs = pl.ds(pl.multiple_of(peer * own, own), own)
+    wide = hidden_ref[...].astype(jnp.float32)
+    for l in range(layers):
+        scaled = (wide * norm_gain_ref[l : l + 1, :]).astype(jnp.bfloat16)
+        squares = jnp.sum(wide * wide, axis=1, keepdims=True)
+        for one in loads[l][:3]:
+            one.wait()
+        part_a[l, :, 0:small] = jnp.dot(scaled, small_v[l], preferred_element_type=jnp.float32)
+        part_a[l, :, small : small + 128] = jnp.broadcast_to(squares, (rows, 128))
+        if first:
+            pl.semaphore_wait(barrier, tp)
+            first = False
+        send_a = to_peer(part_a.at[l, theirs], got_a.at[l], 3 * l)
+        send_a.start()
+        loads[l][3].wait()
+        part_b[l, :, 0:inner] = jnp.dot(scaled, inner_v[l], preferred_element_type=jnp.float32)
+        loads[l][4].wait()
+        part_b[l, :, inner : 2 * inner] = jnp.dot(
+            scaled, gate_v[l], preferred_element_type=jnp.float32
+        )
+        send_b = to_peer(part_b.at[l, theirs], got_b.at[l], 3 * l + 1)
+        send_b.start()
+        send_a.wait()
+        sum_a = part_a[l, mine, :] + got_a[l]
+        factor = lax.rsqrt(sum_a[:, small : small + 1] / total_width + eps)
+        raw_a = (sum_a[:, 0:small] * factor).astype(jnp.bfloat16).astype(jnp.float32)
+        raw_ref[l, :, inner : inner + 2 * cols] = raw_a[:, 0 : 2 * cols]
+        tapped = (
+            pre_ref[l, :, inner : inner + 2 * cols]
+            + raw_a[:, 0 : 2 * cols] * tap_ref[l : l + 1, inner : inner + 2 * cols]
+        )
+        tapped = tapped * jax.nn.sigmoid(tapped)
+        gath[l, t] = jnp.concatenate([tapped[:, :cols], tapped[:, cols:]], axis=0).astype(
+            jnp.bfloat16
+        )
+        spread_start(lambda to: gath.at[l, t], gath.at[l], gath_send.at[l], gath_recv.at[l])
+        step_raw = raw_a[:, 2 * cols :]
+        step = (
+            jnp.dot(
+                jnp.concatenate([step_raw, step_raw], axis=0).astype(jnp.bfloat16),
+                spread_v[...],
+                preferred_element_type=jnp.float32,
+            )[:own]
+            + bias_w[l]
+        )
+        step = jnp.maximum(step, 0.0) + jnp.log1p(jnp.exp(-jnp.abs(step)))
+        retain = jnp.exp(-step * rate_w[l])
+        retain_ref[l] = retain
+        send_b.wait()
+        raw_b = (
+            ((part_b[l, mine, :] + got_b[l]) * factor).astype(jnp.bfloat16).astype(jnp.float32)
+        )
+        raw_ref[l, :, 0:inner] = raw_b[:, 0:inner]
+        act = pre_ref[l, :, 0:inner] + raw_b[:, 0:inner] * tap_ref[l : l + 1, 0:inner]
+        act = act * jax.nn.sigmoid(act)
+        gate = raw_b[:, inner:]
+        gate = gate * jax.nn.sigmoid(gate)
+        grown = step * act
+        scaled_ref[l] = grown
+        loads[l][5].wait()
+        spread_wait(lambda to: gath.at[l, t], gath.at[l], gath_send.at[l], gath_recv.at[l])
+        both = jnp.dot(
+            jnp.concatenate([gath[l, k] for k in range(tp)], axis=1),
+            pick_v[...],
+            preferred_element_type=jnp.float32,
+        )
+        vec_ref[l] = both[:own]
+        overlap = jnp.sum(both[:own] * both[own:], axis=1, keepdims=True)
+        low = both.astype(jnp.bfloat16)
+        carried = jnp.zeros((own, inner), jnp.float32)
+        for b in range(own):
+            held = rec_v[l, b].reshape(inner, rec_v.shape[-1]).astype(jnp.bfloat16)
+            row = lax.dot_general(
+                low, held, (((1,), (1,)), ((), ())), preferred_element_type=jnp.float32
+            )
+            carried = jnp.where(own_row == b, row[own:], carried)
+        gated = (retain * carried + grown * overlap + skip_w[l] * act) * gate
+        group = jnp.sum(gated * gated, axis=1, keepdims=True) / inner
+        normed = gated * lax.rsqrt(group + eps) * group_gain_ref[l : l + 1, :]
+        normed_mine[l] = normed
+        send_c = to_peer(normed_mine.at[l], normed_peer.at[l], 3 * l + 2)
+        send_c.start()
+        loads[l][6].wait()
+        send_c.wait()
+        other = normed_peer[l]
+        lower = me == 0
+        left = jnp.concatenate(
+            [jnp.where(lower, normed, other), jnp.where(lower, other, normed)], axis=0
+        ).astype(jnp.bfloat16)
+        branch = jnp.dot(left, out_v[l], preferred_element_type=jnp.float32).astype(jnp.bfloat16)
+        for k in range(tp):
+            branch_v[l, k] = branch[:, k * chunk : (k + 1) * chunk]
+        spread_start(lambda to: branch_v.at[l, to], red.at[l], red_send.at[l], red_recv.at[l])
+        red[l, t] = branch_v[l, t]
+        spread_wait(lambda to: branch_v.at[l, to], red.at[l], red_send.at[l], red_recv.at[l])
+        total = red[l, 0].astype(jnp.float32)
+        for k in range(1, tp):
+            total = total + red[l, k].astype(jnp.float32)
+        if l == 0:
+            before = hidden_ref[:, pl.ds(pl.multiple_of(t * chunk, chunk), chunk)]
+        else:
+            before = stream_v[l - 1, t]
+        stream_v[l, t] = (total + before.astype(jnp.float32)).astype(jnp.bfloat16)
+        spread_start(lambda to: stream_v.at[l, t], stream_v.at[l], str_send.at[l], str_recv.at[l])
+        spread_wait(lambda to: stream_v.at[l, t], stream_v.at[l], str_send.at[l], str_recv.at[l])
+        after = jnp.concatenate([stream_v[l, k] for k in range(tp)], axis=1)
+        if l == layers - 1:
+            result_ref[...] = after
+        else:
+            wide = after.astype(jnp.float32)
+
+
+def fused_local(
+    hidden,
+    norm_gain,
+    gate_weight,
+    inner_weight,
+    write_weight,
+    read_weight,
+    step_weight,
+    conv_inner,
+    conv_write,
+    conv_read,
+    step_bias,
+    decay_log,
+    skip_gain,
+    group_gain,
+    out_weight,
+    state_inner,
+    state_write,
+    state_read,
+    recurrent,
+):
+    tp = lax.axis_size("tp")
+    layers, width, inner = gate_weight.shape
+    cols = write_weight.shape[2]
+    step_cols = step_weight.shape[2]
+    rows = hidden.shape[0]
+    own, heads, head_dim, state_dim = recurrent.shape[1:]
+    chunk = width // tp
+    taps = jnp.concatenate([conv_inner, conv_write, conv_read], axis=2).astype(jnp.float32)
+    held = jnp.concatenate([state_inner, state_write, state_read], axis=3).astype(jnp.float32)
+    pre = jnp.sum(held * taps[:, None, :-1], axis=2)
+    vmem = pl.BlockSpec(memory_space=pltpu.VMEM)
+    hbm = pl.BlockSpec(memory_space=pl.ANY)
+    f32, bf16 = jnp.float32, jnp.bfloat16
+    dma = pltpu.SemaphoreType.DMA
+    small = 2 * cols + step_cols
+    result, raw, retain, grown, vec = pl.pallas_call(
+        lambda *refs: fused_kernel(tp, *refs),
+        out_shape=(
+            jax.ShapeDtypeStruct((rows, width), bf16),
+            jax.ShapeDtypeStruct((layers, own, inner + 2 * cols), f32),
+            jax.ShapeDtypeStruct((layers, own, inner), f32),
+            jax.ShapeDtypeStruct((layers, own, inner), f32),
+            jax.ShapeDtypeStruct((layers, own, state_dim), f32),
+        ),
+        in_specs=[vmem] * 8 + [hbm] * 7,
+        out_specs=(vmem,) * 5,
+        scratch_shapes=[
+            pltpu.VMEM((layers, width, inner), bf16),
+            pltpu.VMEM((layers, width, inner), bf16),
+            pltpu.VMEM((layers, width, small), bf16),
+            pltpu.VMEM((layers, inner, width), bf16),
+            pltpu.VMEM((layers, own, heads, head_dim, state_dim), f32),
+            pltpu.VMEM((tp * cols, state_dim), bf16),
+            pltpu.VMEM((step_cols, inner), bf16),
+            pltpu.VMEM((layers, rows, small + 128), f32),
+            pltpu.VMEM((layers, rows, 2 * inner), f32),
+            pltpu.VMEM((layers, own, small + 128), f32),
+            pltpu.VMEM((layers, own, 2 * inner), f32),
+            pltpu.VMEM((layers, tp, 2 * own, cols), bf16),
+            pltpu.VMEM((layers, own, inner), f32),
+            pltpu.VMEM((layers, own, inner), f32),
+            pltpu.VMEM((layers, tp, rows, chunk), bf16),
+            pltpu.VMEM((layers, tp, rows, chunk), bf16),
+            pltpu.VMEM((layers, tp, rows, chunk), bf16),
+            dma((7 * layers,)),
+            dma((3 * layers,)),
+            dma((3 * layers,)),
+        ]
+        + [dma((layers, tp))] * 6,
+        compiler_params=pltpu.CompilerParams(
+            collective_id=0, has_side_effects=True, vmem_limit_bytes=56 * 1024 * 1024
+        ),
+    )(
+        hidden,
+        norm_gain,
+        taps[:, -1],
+        pre,
+        step_bias,
+        decay_log,
+        skip_gain,
+        group_gain,
+        gate_weight,
+        inner_weight,
+        write_weight,
+        read_weight,
+        step_weight,
+        out_weight,
+        recurrent,
+    )
+    fresh = raw.astype(jnp.bfloat16)[:, :, None, :]
+    ends = (0, inner, inner + cols, inner + 2 * cols)
+    nexts = [
+        jnp.concatenate([state[:, :, 1:], fresh[..., a:b]], axis=2)
+        for state, a, b in zip((state_inner, state_write, state_read), ends, ends[1:])
+    ]
+    split = (layers, own, heads, head_dim, 1)
+    updated = (
+        retain.reshape(split) * recurrent + grown.reshape(split) * vec[:, :, None, None, :]
+    )
+    return (result, nexts[0], nexts[1], nexts[2], updated)
+
+
 def solution(mesh):
+    tp = mesh.shape["tp"]
+    fits = mesh.shape["dp"] == 2 and tp == GROUPS
     return jax.shard_map(
-        local,
+        fused_local if fits else local,
         mesh=mesh,
         in_specs=(
             P(None, "dp"),

time: 510 us -> 60.2 us (0.12)
  blocking collectives: 245 us -> 0 us
  waiting for transfers between devices: 198 us -> 0 us
  Pallas kernels: 0 us -> 45.3 us
  matrix products: 26.6 us -> 0 us
  between operations: 15.3 us -> 0.71 us
  other arithmetic: 19.8 us -> 9.18 us
    psum x2 -> x0, waiting for transfers between devices: 198 us -> none  [total_over(): return lax.psum(branch, 'tp')]
    all_gather x6 -> x0, blocking collectives: 156 us -> none  [the longest x2 81.1 us: mixer_block(): lax.all_gather(write_act.astype(jnp.bfloat16), 'tp', axis=1, tiled=True)]
    psum x4 -> x0, blocking collectives: 82.8 us -> none  [the longest x2 77.7 us: mixer_block(): lax.psum(jnp.sum(gated_out * gated_out, axis=1)[:, None] * selector[None,...]
    pallas_call x0 -> x1, Pallas kernels: none -> 45.3 us  [fused_local(): pl.pallas_call(lambda *refs: fused_kernel(tp, *refs), out_shape=(jax.Shap...]
    dot_general x14 -> x0, matrix products: 26.6 us -> none  [the longest x10 14.2 us: partial_of(): jnp.dot(normed, weight[number], preferred_element_type=jnp.float32)]
    unnamed x2 -> x0, blocking collectives: 6.75 us -> none
    another operation x10 -> x0, other arithmetic: 5.91 us -> none  [local(): jnp.stack([earlier, later])]
  transfers between devices with their start and end apart: 6 -> 0, of which waited for: 2 -> 0; matrix products, arithmetic and copies ran while one was open for 5% -> 0% of each run, Pallas kernels for 0% -> 0%
where the time goes in v1:
time: 60.2 us; the launch traced here: 59.6 us
  Pallas kernels  45.3 us (75%)
  other arithmetic  9.18 us (15%)
  local copies, waits for them, and re-layouts  4.41 us (7%)
  between operations  0.71 us (1%)
    pallas_call x1, Pallas kernels, fused_local(): pl.pallas_call(lambda *refs: fused_kernel(tp, *refs), out_shape=(jax.Shap...  45.3 us
    add x1, other arithmetic, fused_local(): retain.reshape(split) * recurrent  5.85 us
    unnamed x8, local copies, waits for them, and re-layouts  2.71 us
    reduce_sum x1, other arithmetic, fused_local(): pre = jnp.sum(held * taps[:, None, :-1], axis=2)  1.48 us
    concatenate x2, other arithmetic, fused_local(): jnp.concatenate([state[:, :, 1:], fresh[..., a:b]], axis=2)  1.24 us

profile of v1, /device:TPU:0, one launch (start us, length us, event | category | flops | bytes accessed | tf_op | source)
XLA Modules:
  0.0 59.6 jit_solution(11731394797001365880)
XLA Ops:
  0.6 0.7 %copy.24 = bf16[2,4,512]{2,0,1:T(2,128)(2,1)S(1)} copy(bf16[2,4,512]{2,1,0:T(4,128)(2,1)} %param.26) | data formatting | bytes 16384 | tf_op args[7]
  1.3 0.7 %copy.25 = bf16[2,4,128]{2,0,1:T(2,128)(2,1)S(1)} copy(bf16[2,4,128]{2,1,0:T(4,128)(2,1)} %param.27) | data formatting | bytes 4096 | tf_op args[8]
  2.0 0.7 %copy.26 = bf16[2,4,128]{2,0,1:T(2,128)(2,1)S(1)} copy(bf16[2,4,128]{2,1,0:T(4,128)(2,1)} %param.28) | data formatting | bytes 4096 | tf_op args[9]
  2.7 1.5 %multiply_reduce_fusion.refs_3_ = f32[2,8,768]{2,1,0:T(8,128)} fusion(bf16[2,8,3,128]{3,1,2,0:T(8,128)(2,1)} %param.36, bf16[2,8,3,128]{3,1,2,0:T(8,128)(2,1)} %param.35, bf16[2,8,3,512]{3,1,2,0:T(8,128)(2,1)} %param.34, f32[2,3,768]{2,1,0:T(4,128)S(1)} %copy.27), kind=kLoop, calls=%fused_computation.1 | loop fusion | flops 282624 | bytes 141312 | tf_op jit(solution)/shard_map/reduce_sum | solution.py:467
  4.2 0.6 %convert_bitcast_fusion.1.refs_2_ = f32[2,768]{1,0:T(2,128)} fusion(bf16[2,4,128]{2,0,1:T(2,128)(2,1)S(1)} %copy.26, bf16[2,4,128]{2,0,1:T(2,128)(2,1)S(1)} %copy.25, bf16[2,4,512]{2,0,1:T(2,128)(2,1)S(1)} %copy.24), kind=kLoop, calls=%fused_computation.10 | loop fusion | flops 9216 | bytes 18432 | tf_op jit(solution)/shard_map/squeeze | solution.py:513
  4.8 45.3 %shard_map.218 = (bf16[16,2048]{1,0:T(8,128)(2,1)}, f32[2,8,768]{2,1,0:T(8,128)}, f32[2,8,512]{2,1,0:T(8,128)}, f32[2,8,512]{2,1,0:T(8,128)}, f32[2,8,128]{2,1,0:T(8,128)}) custom-call(bf16[16,2048]{1,0:T(8,128)(2,1)} %refs_0_.1, f32[2,2048]{1,0:T(2,128)} %refs_1_.1, f32[2,768]{1,0:T(2,128)} %convert_bitcast_fusion.1.refs_2_, ...), custom_call_target="tpu_custom_call" | custom-call | tf_op jit(solution)/shard_map/pallas_call | solution.py:473
  50.2 0.8 %mul.35 = f32[2,8,8,64]{3,2,1,0:T(8,128)S(1)} reshape(f32[2,8,512]{2,1,0:T(8,128)} %get-tuple-element.12) | data formatting | bytes 65536 | tf_op jit(solution)/shard_map/mul | solution.py:535
  51.0 0.8 %mul.38 = f32[2,8,8,64]{3,2,1,0:T(8,128)S(1)} reshape(f32[2,8,512]{2,1,0:T(8,128)} %get-tuple-element.13) | data formatting | bytes 65536 | tf_op jit(solution)/shard_map/mul | solution.py:535
  51.8 0.0 copy-start.1
  51.8 0.0 slice-start.1
  51.8 0.0 slice-start.2
  51.9 0.0 slice-start
  51.9 0.0 copy-start
  51.9 5.9 %multiply_add_fusion = f32[2,8,8,64,128]{4,3,2,1,0:T(8,128)} fusion(f32[2,8,8,64,128]{4,3,2,1,0:T(8,128)} %refs_14_.1, f32[2,8,128]{2,1,0:T(8,128)} %get-tuple-element.14, f32[2,8,8,64]{3,2,1,0:T(8,128)S(1)} %mul.38, f32[2,8,8,64]{3,2,1,0:T(8,128)S(1)} %mul.35), kind=kLoop, calls=%fused_computation | loop fusion | flops 3145728 | bytes 8462336 | tf_op jit(solution)/shard_map/add | solution.py:535
  57.7 0.0 copy-done.1
  57.8 0.0 slice-done.1
  57.8 0.0 slice-done.2
  57.8 0.6 %pad_maximum_fusion.1 = (bf16[2,8,3,128]{3,1,2,0:T(8,128)(2,1)}, bf16[2,8,3,128]{3,1,2,0:T(8,128)(2,1)}) fusion(bf16[2,8,1,128]{3,1,2,0:T(8,128)(2,1)S(1)} %get-tuple-element.16, bf16[2,8,2,128]{3,1,2,0:T(8,128)(2,1)S(1)} %slice-done.1, bf16[2,8,1,128]{3,1,2,0:T(8,128)(2,1)S(1)} %get-tuple-element.15, bf16[2,8,2,128]{3,1,2,0:T(8,128)(2,1)S(1)} %slice-done.2), kind=kLoop, calls=%fused_computation.5 | loop fusion | flops 12288 | bytes 49152 | tf_op jit(solution)/shard_map/concatenate | solution.py:530
  58.4 0.0 slice-done
  58.4 0.6 %pad_maximum_fusion = bf16[2,8,3,512]{3,1,2,0:T(8,128)(2,1)} fusion(bf16[2,8,1,512]{3,1,2,0:T(8,128)(2,1)S(1)} %slice_bitcast_fusion, bf16[2,8,2,512]{3,1,2,0:T(8,128)(2,1)S(1)} %slice-done), kind=kLoop, calls=%fused_computation.2 | loop fusion | flops 24576 | bytes 98304 | tf_op jit(solution)/shard_map/concatenate | solution.py:530
  59.0 0.0 copy-done
  59.0 0.6 %copy.32 = bf16[16,2048]{1,0:T(8,128)(2,1)} copy(bf16[16,2048]{1,0:T(8,128)(2,1)S(1)} %copy-done) | data formatting | bytes 131072
  (5 shorter events, 0.0 us)
Async XLA Ops:
  51.8 5.9 %copy-start.1 = (f32[2,8,768]{2,1,0:T(8,128)S(1)}, f32[2,8,768]{2,1,0:T(8,128)}, u32[]{:S(2)}) copy-start(f32[2,8,768]{2,1,0:T(8,128)} %get-tuple-element.11) | copy-start | bytes 147460
  51.8 5.9 %slice-start.1 = ((bf16[2,8,3,128]{3,1,2,0:T(8,128)(2,1)}), bf16[2,8,2,128]{3,1,2,0:T(8,128)(2,1)S(1)}, s32[]{:S(2)}) async-start(bf16[2,8,3,128]{3,1,2,0:T(8,128)(2,1)} %param.35), calls=%async_computation.1 | async-start | bytes 16384 | tf_op jit(solution)/shard_map/slice | solution.py:530
  51.8 5.9 %slice-start.2 = ((bf16[2,8,3,128]{3,1,2,0:T(8,128)(2,1)}), bf16[2,8,2,128]{3,1,2,0:T(8,128)(2,1)S(1)}, s32[]{:S(2)}) async-start(bf16[2,8,3,128]{3,1,2,0:T(8,128)(2,1)} %param.36), calls=%async_computation.2 | async-start | bytes 16384 | tf_op jit(solution)/shard_map/slice | solution.py:530
  51.9 6.5 %slice-start = ((bf16[2,8,3,512]{3,1,2,0:T(8,128)(2,1)}), bf16[2,8,2,512]{3,1,2,0:T(8,128)(2,1)S(1)}, s32[]{:S(2)}) async-start(bf16[2,8,3,512]{3,1,2,0:T(8,128)(2,1)} %param.34), calls=%async_computation | async-start | bytes 65536 | tf_op jit(solution)/shard_map/slice | solution.py:530
  51.9 7.2 %copy-start = (bf16[16,2048]{1,0:T(8,128)(2,1)S(1)}, bf16[16,2048]{1,0:T(8,128)(2,1)}, u32[]{:S(2)}) copy-start(bf16[16,2048]{1,0:T(8,128)(2,1)} %get-tuple-element.24) | copy-start | bytes 196612

commit v2 on v1

--- a/solution.py
+++ b/solution.py
@@ -169,8 +169,12 @@
     tp,
     hidden_ref,
     norm_gain_ref,
-    tap_ref,
-    pre_ref,
+    conv_i_ref,
+    conv_w_ref,
+    conv_r_ref,
+    state_i_ref,
+    state_w_ref,
+    state_r_ref,
     bias_ref,
     decay_ref,
     skip_ref,
@@ -183,10 +187,10 @@
     out_hbm,
     rec_hbm,
     result_ref,
-    raw_ref,
-    retain_ref,
-    scaled_ref,
-    vec_ref,
+    fresh_i_ref,
+    fresh_w_ref,
+    fresh_r_ref,
+    updated_hbm,
     gate_v,
     inner_v,
     small_v,
@@ -204,7 +208,9 @@
     branch_v,
     red,
     stream_v,
+    turned_v,
     w_sem,
+    u_sem,
     dp_send,
     dp_recv,
     gath_send,
@@ -247,9 +253,8 @@
                 load(out_hbm.at[l], out_v.at[l], at + 6),
             ]
         )
-    for l in range(layers):
-        for one in loads[l]:
-            one.start()
+    for one in loads[0]:
+        one.start()
 
     barrier = pltpu.get_barrier_semaphore()
 
@@ -293,6 +298,14 @@
             recv_sem=dp_recv.at[number],
             device_id={"tp": t, "dp": peer},
         )
+
+    def earlier_taps(state_ref, conv_ref, l):
+        taps = conv_ref[l].astype(jnp.float32)
+        count = state_ref.shape[1]
+        total = state_ref[l, 0].astype(jnp.float32) * taps[0:1]
+        for k in range(1, count):
+            total = total + state_ref[l, k].astype(jnp.float32) * taps[k : k + 1]
+        return total, taps[count : count + 1]
 
     def spread_start(source_of, target, sends, recvs):
         @pl.loop(1, tp)
@@ -336,6 +349,9 @@
             first = False
         send_a = to_peer(part_a.at[l, theirs], got_a.at[l], 3 * l)
         send_a.start()
+        if l + 1 < layers:
+            for one in loads[l + 1]:
+                one.start()
         loads[l][3].wait()
         part_b[l, :, 0:inner] = jnp.dot(scaled, inner_v[l], preferred_element_type=jnp.float32)
         loads[l][4].wait()
@@ -344,19 +360,22 @@
         )
         send_b = to_peer(part_b.at[l, theirs], got_b.at[l], 3 * l + 1)
         send_b.start()
+        pre_w = earlier_taps(state_w_ref, conv_w_ref, l)
+        pre_r = earlier_taps(state_r_ref, conv_r_ref, l)
+        pre_i = earlier_taps(state_i_ref, conv_i_ref, l)
         send_a.wait()
         sum_a = part_a[l, mine, :] + got_a[l]
         factor = lax.rsqrt(sum_a[:, small : small + 1] / total_width + eps)
         raw_a = (sum_a[:, 0:small] * factor).astype(jnp.bfloat16).astype(jnp.float32)
-        raw_ref[l, :, inner : inner + 2 * cols] = raw_a[:, 0 : 2 * cols]
-        tapped = (
-            pre_ref[l, :, inner : inner + 2 * cols]
-            + raw_a[:, 0 : 2 * cols] * tap_ref[l : l + 1, inner : inner + 2 * cols]
-        )
-        tapped = tapped * jax.nn.sigmoid(tapped)
-        gath[l, t] = jnp.concatenate([tapped[:, :cols], tapped[:, cols:]], axis=0).astype(
-            jnp.bfloat16
-        )
+        acts = []
+        for fresh_ref, (early, tap), raw in (
+            (fresh_w_ref, pre_w, raw_a[:, 0:cols]),
+            (fresh_r_ref, pre_r, raw_a[:, cols : 2 * cols]),
+        ):
+            fresh_ref[l] = raw.astype(jnp.bfloat16)
+            tapped = early + raw * tap
+            acts.append(tapped * jax.nn.sigmoid(tapped))
+        gath[l, t] = jnp.concatenate(acts, axis=0).astype(jnp.bfloat16)
         spread_start(lambda to: gath.at[l, t], gath.at[l], gath_send.at[l], gath_recv.at[l])
         step_raw = raw_a[:, 2 * cols :]
         step = (
@@ -369,34 +388,30 @@
         )
         step = jnp.maximum(step, 0.0) + jnp.log1p(jnp.exp(-jnp.abs(step)))
         retain = jnp.exp(-step * rate_w[l])
-        retain_ref[l] = retain
         send_b.wait()
         raw_b = (
             ((part_b[l, mine, :] + got_b[l]) * factor).astype(jnp.bfloat16).astype(jnp.float32)
         )
-        raw_ref[l, :, 0:inner] = raw_b[:, 0:inner]
-        act = pre_ref[l, :, 0:inner] + raw_b[:, 0:inner] * tap_ref[l : l + 1, 0:inner]
+        fresh_i_ref[l] = raw_b[:, 0:inner].astype(jnp.bfloat16)
+        act = pre_i[0] + raw_b[:, 0:inner] * pre_i[1]
         act = act * jax.nn.sigmoid(act)
         gate = raw_b[:, inner:]
         gate = gate * jax.nn.sigmoid(gate)
         grown = step * act
-        scaled_ref[l] = grown
         loads[l][5].wait()
+        for b in range(own):
+            turned_v[b] = rec_v[l, b].reshape(inner, rec_v.shape[-1]).T.astype(jnp.bfloat16)
         spread_wait(lambda to: gath.at[l, t], gath.at[l], gath_send.at[l], gath_recv.at[l])
         both = jnp.dot(
             jnp.concatenate([gath[l, k] for k in range(tp)], axis=1),
             pick_v[...],
             preferred_element_type=jnp.float32,
         )
-        vec_ref[l] = both[:own]
         overlap = jnp.sum(both[:own] * both[own:], axis=1, keepdims=True)
         low = both.astype(jnp.bfloat16)
         carried = jnp.zeros((own, inner), jnp.float32)
         for b in range(own):
-            held = rec_v[l, b].reshape(inner, rec_v.shape[-1]).astype(jnp.bfloat16)
-            row = lax.dot_general(
-                low, held, (((1,), (1,)), ((), ())), preferred_element_type=jnp.float32
-            )
+            row = jnp.dot(low, turned_v[b], preferred_element_type=jnp.float32)
             carried = jnp.where(own_row == b, row[own:], carried)
         gated = (retain * carried + grown * overlap + skip_w[l] * act) * gate
         group = jnp.sum(gated * gated, axis=1, keepdims=True) / inner
@@ -416,6 +431,12 @@
             branch_v[l, k] = branch[:, k * chunk : (k + 1) * chunk]
         spread_start(lambda to: branch_v.at[l, to], red.at[l], red_send.at[l], red_recv.at[l])
         red[l, t] = branch_v[l, t]
+        turned = jnp.concatenate([retain, grown], axis=0).T
+        for b in range(own):
+            state = rec_v[l, b].reshape(inner, rec_v.shape[-1])
+            state = turned[:, b : b + 1] * state + turned[:, own + b : own + b + 1] * both[b : b + 1]
+            rec_v[l, b] = state.reshape(rec_v.shape[2:])
+        pltpu.make_async_copy(rec_v.at[l], updated_hbm.at[l], u_sem.at[l]).start()
         spread_wait(lambda to: branch_v.at[l, to], red.at[l], red_send.at[l], red_recv.at[l])
         total = red[l, 0].astype(jnp.float32)
         for k in range(1, tp):
@@ -432,6 +453,8 @@
             result_ref[...] = after
         else:
             wide = after.astype(jnp.float32)
+    for l in range(layers):
+        pltpu.make_async_copy(rec_v.at[l], updated_hbm.at[l], u_sem.at[l]).wait()
 
 
 def fused_local(
@@ -462,25 +485,22 @@
     rows = hidden.shape[0]
     own, heads, head_dim, state_dim = recurrent.shape[1:]
     chunk = width // tp
-    taps = jnp.concatenate([conv_inner, conv_write, conv_read], axis=2).astype(jnp.float32)
-    held = jnp.concatenate([state_inner, state_write, state_read], axis=3).astype(jnp.float32)
-    pre = jnp.sum(held * taps[:, None, :-1], axis=2)
     vmem = pl.BlockSpec(memory_space=pltpu.VMEM)
     hbm = pl.BlockSpec(memory_space=pl.ANY)
     f32, bf16 = jnp.float32, jnp.bfloat16
     dma = pltpu.SemaphoreType.DMA
     small = 2 * cols + step_cols
-    result, raw, retain, grown, vec = pl.pallas_call(
+    result, *fresh, updated = pl.pallas_call(
         lambda *refs: fused_kernel(tp, *refs),
         out_shape=(
             jax.ShapeDtypeStruct((rows, width), bf16),
-            jax.ShapeDtypeStruct((layers, own, inner + 2 * cols), f32),
-            jax.ShapeDtypeStruct((layers, own, inner), f32),
-            jax.ShapeDtypeStruct((layers, own, inner), f32),
-            jax.ShapeDtypeStruct((layers, own, state_dim), f32),
-        ),
-        in_specs=[vmem] * 8 + [hbm] * 7,
-        out_specs=(vmem,) * 5,
+            jax.ShapeDtypeStruct((layers, own, inner), bf16),
+            jax.ShapeDtypeStruct((layers, own, cols), bf16),
+            jax.ShapeDtypeStruct((layers, own, cols), bf16),
+            jax.ShapeDtypeStruct(recurrent.shape, f32),
+        ),
+        in_specs=[vmem] * 12 + [hbm] * 7,
+        out_specs=(vmem,) * 4 + (hbm,),
         scratch_shapes=[
             pltpu.VMEM((layers, width, inner), bf16),
             pltpu.VMEM((layers, width, inner), bf16),
@@ -499,7 +519,9 @@
             pltpu.VMEM((layers, tp, rows, chunk), bf16),
             pltpu.VMEM((layers, tp, rows, chunk), bf16),
             pltpu.VMEM((layers, tp, rows, chunk), bf16),
+            pltpu.VMEM((own, state_dim, inner), bf16),
             dma((7 * layers,)),
+            dma((layers,)),
             dma((3 * layers,)),
             dma((3 * layers,)),
         ]
@@ -510,8 +532,12 @@
     )(
         hidden,
         norm_gain,
-        taps[:, -1],
-        pre,
+        conv_inner,
+        conv_write,
+        conv_read,
+        jnp.swapaxes(state_inner, 1, 2),
+        jnp.swapaxes(state_write, 1, 2),
+        jnp.swapaxes(state_read, 1, 2),
         step_bias,
         decay_log,
         skip_gain,
@@ -524,16 +550,10 @@
         out_weight,
         recurrent,
     )
-    fresh = raw.astype(jnp.bfloat16)[:, :, None, :]
-    ends = (0, inner, inner + cols, inner + 2 * cols)
     nexts = [
-        jnp.concatenate([state[:, :, 1:], fresh[..., a:b]], axis=2)
-        for state, a, b in zip((state_inner, state_write, state_read), ends, ends[1:])
+        jnp.concatenate([state[:, :, 1:], new[:, :, None]], axis=2)
+        for state, new in zip((state_inner, state_write, state_read), fresh)
     ]
-    split = (layers, own, heads, head_dim, 1)
-    updated = (
-        retain.reshape(split) * recurrent + grown.reshape(split) * vec[:, :, None, None, :]
-    )
     return (result, nexts[0], nexts[1], nexts[2], updated)
 
 

time: 60.2 us -> 55.2 us (0.917)
  other arithmetic: 9.18 us -> 2.64 us
  local copies, waits for them, and re-layouts: 4.41 us -> 6.28 us
    add x1 -> x0, other arithmetic: 5.85 us -> none  [fused_local(): retain.reshape(split) * recurrent]
    unnamed x8, local copies, waits for them, and re-layouts: 2.71 us -> 6.27 us
    mul x2 -> x0, local copies, waits for them, and re-layouts: 1.67 us -> none  [the longest x1 0.84 us: fused_local(): retain.reshape(split) * recurrent]
    reduce_sum x1 -> x0, other arithmetic: 1.48 us -> none  [fused_local(): pre = jnp.sum(held * taps[:, None, :-1], axis=2)]
    concatenate x2, other arithmetic: 1.24 us -> 2.64 us  [fused_local(): jnp.concatenate([state[:, :, 1:], new[:, :, None]], axis=2)]
where the time goes in v2:
time: 55.2 us; the launch traced here: 54.8 us
  Pallas kernels  45.2 us (82%)
  local copies, waits for them, and re-layouts  6.28 us (11%)
  other arithmetic  2.64 us (5%)
  between operations  0.71 us (1%)
    pallas_call x1, Pallas kernels, fused_local(): pl.pallas_call(lambda *refs: fused_kernel(tp, *refs), out_shape=(jax.Shap...  45.2 us
    unnamed x8, local copies, waits for them, and re-layouts  6.27 us
    concatenate x2, other arithmetic, fused_local(): jnp.concatenate([state[:, :, 1:], new[:, :, None]], axis=2)  2.64 us

profile of v2, /device:TPU:0, one launch (start us, length us, event | category | flops | bytes accessed | tf_op | source)
XLA Modules:
  0.0 54.8 jit_solution(17743357100892603824)
XLA Ops:
  0.6 0.0 copy-start.1
  0.6 0.0 copy-start.2
  0.7 0.0 copy-start
  0.7 45.2 %shard_map.218 = (bf16[16,2048]{1,0:T(8,128)(2,1)}, bf16[2,8,512]{2,1,0:T(8,128)(2,1)}, bf16[2,8,128]{2,1,0:T(8,128)(2,1)}, bf16[2,8,128]{2,1,0:T(8,128)(2,1)}, f32[2,8,8,64,128]{4,3,2,1,0:T(8,128)}) custom-call(bf16[16,2048]{1,0:T(8,128)(2,1)} %refs_0_.1, f32[2,2048]{1,0:T(2,128)} %refs_1_.1, bf16[2,4,512]{2,1,0:T(4,128)(2,1)} %refs_2_.1, ...), custom_call_target="tpu_custom_call" | custom-call | tf_op jit(solution)/shard_map/pallas_call | solution.py:493
  45.9 0.0 copy-done.1
  45.9 0.0 copy-done.2
  45.9 1.3 %pad_maximum_fusion.1 = (bf16[2,8,3,128]{3,1,2,0:T(8,128)(2,1)}, bf16[2,8,3,128]{3,1,2,0:T(8,128)(2,1)}) fusion(bf16[2,8,1,128]{3,1,2,0:T(8,128)(2,1)} %bitcast.16, bf16[2,8,2,128]{3,1,2,0:T(8,128)(2,1)S(1)} %slice.10, bf16[2,8,1,128]{3,1,2,0:T(8,128)(2,1)} %bitcast.17, bf16[2,8,2,128]{3,1,2,0:T(8,128)(2,1)S(1)} %slice.11), kind=kLoop, calls=%fused_computation.1 | loop fusion | flops 12288 | bytes 49152 | tf_op jit(solution)/shard_map/concatenate | solution.py:554
  47.2 0.0 copy-done
  47.2 1.3 %pad_maximum_fusion = bf16[2,8,3,512]{3,1,2,0:T(8,128)(2,1)} fusion(bf16[2,8,1,512]{3,1,2,0:T(8,128)(2,1)} %bitcast.15, bf16[2,8,2,512]{3,1,2,0:T(8,128)(2,1)S(1)} %slice.9), kind=kLoop, calls=%fused_computation | loop fusion | flops 24576 | bytes 98304 | tf_op jit(solution)/shard_map/concatenate | solution.py:554
  48.6 1.5 %copy.29 = bf16[16,2048]{1,0:T(8,128)(2,1)} copy(bf16[16,2048]{1,0:T(8,128)(2,1)} %get-tuple-element.22) | data formatting | bytes 131072
  50.0 4.8 %copy.30 = f32[2,8,8,64,128]{4,3,2,1,0:T(8,128)} copy(f32[2,8,8,64,128]{4,3,2,1,0:T(8,128)} %get-tuple-element.26) | data formatting | bytes 8388608
  (3 shorter events, 0.0 us)
Async XLA Ops:
  0.6 45.2 %copy-start.1 = (bf16[2,8,3,128]{3,1,2,0:T(8,128)(2,1)S(1)}, bf16[2,8,3,128]{3,1,2,0:T(8,128)(2,1)}, u32[]{:S(2)}) copy-start(bf16[2,8,3,128]{3,1,2,0:T(8,128)(2,1)} %param.35) | copy-start | bytes 36868
  0.6 45.2 %copy-start.2 = (bf16[2,8,3,128]{3,1,2,0:T(8,128)(2,1)S(1)}, bf16[2,8,3,128]{3,1,2,0:T(8,128)(2,1)}, u32[]{:S(2)}) copy-start(bf16[2,8,3,128]{3,1,2,0:T(8,128)(2,1)} %param.36) | copy-start | bytes 36868
  0.7 46.6 %copy-start = (bf16[2,8,3,512]{3,1,2,0:T(8,128)(2,1)S(1)}, bf16[2,8,3,512]{3,1,2,0:T(8,128)(2,1)}, u32[]{:S(2)}) copy-start(bf16[2,8,3,512]{3,1,2,0:T(8,128)(2,1)} %param.34) | copy-start | bytes 147460
